TPU v7x, 32 devices: a whole 2x2x4 slice. The times are simulated.
32 devices in a mesh: sp: 8 (over z, x), dp: 4 (over y, core).
Axes of the slice: x: 2, y: 2, z: 4, core: 2. Of those that a mesh axis runs over, the one named last changes fastest.
Arguments:
- queries: bfloat16 [4, 1024, 16, 128], P('dp', 'sp'), may hold values from -6 to 6
- key_rows: bfloat16 [4, 1024, 4, 128], P('dp', 'sp'), may hold values from -6 to 6
- values: bfloat16 [4, 1024, 4, 128], P('dp', 'sp'), may hold values from -6 to 6
- query_gain: float32 [128], replicated, may hold values from 0.4 to 5
- key_gain: float32 [128], replicated, may hold values from 0.4 to 5
- out_weight: bfloat16 [2048, 2048], P('sp', 'dp'), may hold values from -0.125 to 0.125
- residual: bfloat16 [4, 1024, 2048], P('dp', 'sp'), may hold values from -6 to 6
- norm_gain: float32 [2048], replicated, may hold values from 0.1 to 1.9
- expert_gate: bfloat16 [8, 2048, 1792], P('sp'), may hold values from -0.125 to 0.125
- expert_up: bfloat16 [8, 2048, 1792], P('sp'), may hold values from -0.125 to 0.125
- expert_down: bfloat16 [8, 1792, 2048], P('sp'), may hold values from -0.125 to 0.125
- routes: int32 [4, 1024, 2], P('dp', 'sp'), may hold values from 0 to 7, all different within a row; in each aligned block of 64 rows (0 to 63, 64 to 127, ..., all dimensions but the last counted through in order) at most 32 rows name the same one
- route_weight: float32 [4, 1024, 2], P('dp', 'sp'), may hold values from 0.25 to 1
Outputs:
- layer_out: bfloat16 [4, 1024, 2048], P('dp', 'sp')
Inputs may be any that keep to these rules, and one draw needn't show every extreme that they name: `routes`: in each aligned block of 64 rows of one device, no expert is named by more than 32 entries, a bound that some block reaches; the two experts of a row differ.
All inputs are finite; a program needn't handle non-finite values.
Results may differ from a plain program's by a relative error of at most 0.0095.
The roundings to bfloat16 on the way count: a program that leaves them out, or rounds other values in their place, can miss the bound.
Values may be sent and summed in bfloat16 or wider, within the bound.
A program may use at most 128 MiB of HBM per device.

v0:
```python
import jax
import jax.numpy as jnp
from jax import lax
from jax.sharding import PartitionSpec as P

GRID_W = 64


EPS = 1e-06
THETA = 10000.0


def rotate_half(vector, position):
    half_size = vector.shape[-1] // 2
    inverse = THETA ** (-jnp.arange(half_size, dtype=jnp.float32) / half_size)
    angles = position[:, None] * inverse[None, :]
    cosine = jnp.cos(angles)[:, None, :]
    sine_part = jnp.sin(angles)[:, None, :]
    first_part = vector[..., :half_size]
    second_part = vector[..., half_size:]
    return jnp.concatenate(
        [
            first_part * cosine - second_part * sine_part,
            first_part * sine_part + second_part * cosine,
        ],
        axis=-1,
    )


def normalize_rotate(vector, gain, positions):
    as_float = vector.astype(jnp.float32)
    scaled = (
        as_float * lax.rsqrt(jnp.mean(as_float * as_float, axis=-1, keepdims=True) + EPS) * gain
    )
    grid_row = (positions // GRID_W).astype(jnp.float32)
    column = (positions % GRID_W).astype(jnp.float32)
    quarter = scaled.shape[-1] // 2
    turned = jnp.concatenate(
        [rotate_half(scaled[..., :quarter], grid_row), rotate_half(scaled[..., quarter:], column)],
        axis=-1,
    )
    return turned.astype(jnp.bfloat16)


def softmax_rows(scores):
    row_max = jnp.max(scores, axis=-1, keepdims=True)
    exponent = jnp.exp(scores - row_max)
    return (exponent / jnp.sum(exponent, axis=-1, keepdims=True)).astype(jnp.bfloat16)


def attend_block(query_rows, key_rows, value_rows):
    scores = jnp.einsum(
        "qd,kd->qk", query_rows, key_rows, preferred_element_type=jnp.float32
    ) * query_rows.shape[-1] ** (-0.5)
    weights = softmax_rows(scores)
    return jnp.dot(weights, value_rows, preferred_element_type=jnp.float32).astype(jnp.bfloat16)


def attend_heads(head_query, head_key, head_value):
    length, head_count, head_width = head_query.shape
    block_size = min(512, length)
    outputs = []
    for head_index in range(head_count):
        key_slice = head_key[:, head_index]
        value_slice = head_value[:, head_index]
        query_blocks = head_query[:, head_index].reshape(
            length // block_size, block_size, head_width
        )

        def one_block(query_block):
            return attend_block(query_block, key_slice, value_slice)

        outputs.append(lax.map(one_block, query_blocks).reshape(length, head_width))
    return jnp.stack(outputs, axis=1)


def project_tokens(attended, out_weight):
    all_rows = lax.all_gather(attended[None], "dp", axis=0, tiled=True)
    local_cols = lax.all_gather(out_weight, "sp", axis=0, tiled=True)
    partial_cols = jnp.einsum(
        "std,dc->stc", all_rows, local_cols, preferred_element_type=jnp.float32
    )
    back_cols = lax.all_to_all(
        partial_cols.astype(jnp.bfloat16), "dp", split_axis=0, concat_axis=2, tiled=True
    ).astype(partial_cols.dtype)
    return back_cols[0]


def on_device(
    queries,
    key_rows,
    values,
    query_gain,
    key_gain,
    out_weight,
    residual,
    norm_gain,
    expert_gate,
    expert_up,
    expert_down,
    routes,
    route_weight,
):
    tok_count = queries.shape[1]
    head_count = queries.shape[2]
    head_width = queries.shape[3]
    group_size = head_count // key_rows.shape[2]
    positions = lax.axis_index("sp") * tok_count + jnp.arange(tok_count, dtype=jnp.int32)
    rot_query = normalize_rotate(queries[0], query_gain, positions)
    rot_key = normalize_rotate(key_rows[0], key_gain, positions)
    value_rows = values[0]
    head_query, head_key, head_value = (
        lax.all_to_all(rot_query, "sp", split_axis=1, concat_axis=0, tiled=True),
        lax.all_to_all(
            jnp.repeat(rot_key, group_size, axis=1), "sp", split_axis=1, concat_axis=0, tiled=True
        ),
        lax.all_to_all(
            jnp.repeat(value_rows, group_size, axis=1),
            "sp",
            split_axis=1,
            concat_axis=0,
            tiled=True,
        ),
    )
    by_heads = attend_heads(head_query, head_key, head_value)
    returned_heads = lax.all_to_all(by_heads, "sp", split_axis=0, concat_axis=1, tiled=True)
    projected = project_tokens(
        returned_heads.reshape(tok_count, head_count * head_width), out_weight
    )
    mixed_sum = residual[0].astype(jnp.float32) + projected
    normed = (
        mixed_sum
        * lax.rsqrt(jnp.mean(mixed_sum * mixed_sum, axis=-1, keepdims=True) + EPS)
        * norm_gain
    ).astype(jnp.bfloat16)
    experts = expert_gate.shape[0] * lax.axis_size("sp")
    half_rows = tok_count // 2
    capacity = max(2, 4 * half_rows // experts)
    chosen = routes[0].reshape(2, half_rows * 2)
    onehot = (chosen[..., None] == jnp.arange(experts, dtype=jnp.int32)).astype(jnp.int32)
    slot_rank = jnp.sum(jnp.cumsum(onehot, axis=1) * onehot, axis=-1) - 1
    slot_index = jnp.arange(2, dtype=jnp.int32)[:, None] * capacity + slot_rank
    target = (chosen * (2 * capacity) + slot_index).reshape(-1)
    model_width = normed.shape[1]
    filled = (
        jnp.zeros((experts * 2 * capacity, model_width), jnp.bfloat16)
        .at[target]
        .set(jnp.repeat(normed, 2, axis=0))
    )
    buffer = filled.reshape(experts, 2 * capacity, model_width)
    slot_batch = lax.all_to_all(buffer, "sp", split_axis=0, concat_axis=0, tiled=True)
    sources, slot_count, feature_count = slot_batch.shape
    flat_rows = slot_batch.reshape(sources * slot_count, feature_count)
    gate_part = jnp.dot(flat_rows, expert_gate[0], preferred_element_type=jnp.float32)
    up_part = jnp.dot(flat_rows, expert_up[0], preferred_element_type=jnp.float32)
    hidden = (jax.nn.silu(gate_part) * up_part).astype(jnp.bfloat16)
    expert_result = jnp.dot(hidden, expert_down[0], preferred_element_type=jnp.float32).astype(
        jnp.bfloat16
    )
    served = expert_result.reshape(sources, slot_count, feature_count)
    returned = lax.all_to_all(served, "sp", split_axis=0, concat_axis=0, tiled=True)
    picked = (
        returned.reshape(-1, model_width)[target]
        .astype(jnp.float32)
        .reshape(tok_count, 2, model_width)
    )
    result = mixed_sum + jnp.sum(picked * route_weight[0][..., None], axis=1)
    return result.astype(jnp.bfloat16)[None]


def solution(mesh):
    in_specs = (
        P("dp", "sp", None, None),
        P("dp", "sp", None, None),
        P("dp", "sp", None, None),
        P(),
        P(),
        P("sp", "dp"),
        P("dp", "sp", None),
        P(),
        P("sp", None, None),
        P("sp", None, None),
        P("sp", None, None),
        P("dp", "sp", None),
        P("dp", "sp", None),
    )
    out_specs = P("dp", "sp", None)
    return jax.shard_map(
        on_device, mesh=mesh, in_specs=in_specs, out_specs=out_specs, check_vma=False
    )
```

profile of v0, /device:TPU:0, one launch (start us, length us, event | category | flops | bytes accessed | tf_op | source)
XLA Modules:
  0.0 305.6 jit_solution(6616813318897419317)
XLA Ops:
  11.2 7.3 %all-to-all-start.1 = ((bf16[128,16,128]{2,0,1:T(8,128)(2,1)}), bf16[128,16,128]{2,0,1:T(8,128)(2,1)S(1)}, u32[]{:S(2)}, u32[]{:S(2)}) async-start(bf16[128,16,128]{2,0,1:T(8,128)(2,1)} %bitcast.12), calls=%async_computation.1 | async-start | bytes 1048576 | tf_op jit(solution)/shard_map/all_to_all | solution.py:114
  20.1 1.5 pad_maximum_fusion
  21.6 11.4 %all-to-all-done.1 = bf16[128,16,128]{2,0,1:T(8,128)(2,1)S(1)} async-done(((bf16[128,16,128]{2,0,1:T(8,128)(2,1)}), bf16[128,16,128]{2,0,1:T(8,128)(2,1)S(1)}, u32[]{:S(2)}, u32[]{:S(2)}) %all-to-all-start.1) | async-done | bytes 524320 | tf_op jit(solution)/shard_map/all_to_all | solution.py:114
  33.0 3.6 %all-to-all-start = ((bf16[128,16,128]{2,0,1:T(8,128)(2,1)}), bf16[128,16,128]{2,0,1:T(8,128)(2,1)S(1)}, u32[]{:S(2)}, u32[]{:S(2)}) async-start(bf16[128,16,128]{2,0,1:T(8,128)(2,1)} %pad_maximum_fusion), calls=%async_computation | async-start | bytes 1048576 | tf_op jit(solution)/shard_map/all_to_all | solution.py:113
  36.7 14.6 %all-to-all-done = bf16[128,16,128]{2,0,1:T(8,128)(2,1)S(1)} async-done(((bf16[128,16,128]{2,0,1:T(8,128)(2,1)}), bf16[128,16,128]{2,0,1:T(8,128)(2,1)S(1)}, u32[]{:S(2)}, u32[]{:S(2)}) %all-to-all-start) | async-done | bytes 524320 | tf_op jit(solution)/shard_map/all_to_all | solution.py:113
  52.2 3.6 %all-to-all-start.2 = ((bf16[128,16,128]{2,0,1:T(8,128)(2,1)}), bf16[128,16,128]{2,0,1:T(8,128)(2,1)S(1)}, u32[]{:S(2)}, u32[]{:S(2)}) async-start(bf16[128,16,128]{2,0,1:T(8,128)(2,1)} %bitcast.18), calls=%async_computation.2 | async-start | bytes 1048576 | tf_op jit(solution)/shard_map/all_to_all | solution.py:117
  56.8 13.7 %all-to-all-done.2 = bf16[128,16,128]{2,0,1:T(8,128)(2,1)S(1)} async-done(((bf16[128,16,128]{2,0,1:T(8,128)(2,1)}), bf16[128,16,128]{2,0,1:T(8,128)(2,1)S(1)}, u32[]{:S(2)}, u32[]{:S(2)}) %all-to-all-start.2) | async-done | bytes 524320 | tf_op jit(solution)/shard_map/all_to_all | solution.py:117
  70.6 3.4 %while.20 = (s32[]{:T(128)}, bf16[2,512,128]{2,1,0:T(8,128)(2,1)S(1)}, bf16[2,512,128]{2,1,0:T(8,128)(2,1)S(1)}, bf16[1024,128]{1,0:T(8,128)(2,1)S(1)}, bf16[1024,128]{1,0:T(8,128)(2,1)S(1)}, /*index=5*/s32[]{:T(128)}) while((s32[]{:T(128)}, bf16[2,512,128]{2,1,0:T(8,128)(2,1)S(1)}, bf16[2,512,128]{2,1,0:T(8,128)(2,1)S(1)}, ...), condition=%wide.region_5.6_spmd, body=%wide.region_2.5_spmd.sunk | while | flops 273218560 | bytes 7088205 | solution.py:73
  74.1 3.5 %while.21 = (s32[]{:T(128)}, bf16[2,512,128]{2,1,0:T(8,128)(2,1)S(1)}, bf16[2,512,128]{2,1,0:T(8,128)(2,1)S(1)}, bf16[1024,128]{1,0:T(8,128)(2,1)S(1)}, bf16[1024,128]{1,0:T(8,128)(2,1)S(1)}, /*index=5*/s32[]{:T(128)}) while((s32[]{:T(128)}, bf16[2,512,128]{2,1,0:T(8,128)(2,1)S(1)}, bf16[2,512,128]{2,1,0:T(8,128)(2,1)S(1)}, ...), condition=%wide.region_9.10_spmd, body=%wide.region_6.9_spmd.sunk | while | flops 273218560 | bytes 7088205 | solution.py:73
  78.2 28.0 %all_to_all.88 = bf16[1024,2,128]{2,1,0:T(2,128)(2,1)S(1)} all-to-all(bf16[1024,2,128]{2,1,0:T(2,128)(2,1)S(1)} %copy.114), channel_id=1, replica_groups=mesh['sp'=8,'dp'=4] {'sp'}, dimensions={0} | all-to-all | bytes 1048576 | tf_op jit(solution)/shard_map/all_to_all | solution.py:126
  108.6 5.1 %all-gather.5.cloned.1.call-done = bf16[2048,512]{1,0:T(8,128)(2,1)} async-done(((bf16[256,512]{1,0:T(8,128)(2,1)}), bf16[2048,512]{1,0:T(8,128)(2,1)}) %all-gather.5.cloned.1.call-update) | async-done | bytes 2097168 | tf_op jit(solution)/shard_map/all_gather | solution.py:79
  113.7 23.2 %all-gather.3.cloned.1.call-done = bf16[4,128,2048]{2,1,0:T(8,128)(2,1)} async-done(((bf16[1,128,2048]{2,1,0:T(8,128)(2,1)}), bf16[4,128,2048]{2,1,0:T(8,128)(2,1)}) %all-gather.3.cloned.1.call-update) | async-done | bytes 2097168 | tf_op jit(solution)/shard_map/all_gather | solution.py:78
  136.9 4.3 %fusion.29 = bf16[4,128,512]{2,1,0:T(8,128)(2,1)} fusion(bf16[4,128,2048]{2,1,0:T(8,128)(2,1)} %all-gather.3.cloned.1.call-done, bf16[2048,512]{1,0:T(8,128)(2,1)} %all-gather.5.cloned.1.call-done), kind=kOutput, calls=%fused_computation.41 | convolution fusion | flops 1074003968 | bytes 4718592 | tf_op jit(solution)/shard_map/std,dc->stc/dot_general | solution.py:80
  141.1 3.7 %all-to-all-start.4 = ((bf16[4,128,512]{2,1,0:T(8,128)(2,1)}), bf16[4,128,512]{2,1,0:T(8,128)(2,1)S(1)}, u32[]{:S(2)}, u32[]{:S(2)}) async-start(bf16[4,128,512]{2,1,0:T(8,128)(2,1)} %fusion.29), calls=%async_computation.4 | async-start | bytes 1048576 | tf_op jit(solution)/shard_map/all_to_all | solution.py:83
  144.9 8.5 %all-to-all-done.4 = bf16[4,128,512]{2,1,0:T(8,128)(2,1)S(1)} async-done(((bf16[4,128,512]{2,1,0:T(8,128)(2,1)}), bf16[4,128,512]{2,1,0:T(8,128)(2,1)S(1)}, u32[]{:S(2)}, u32[]{:S(2)}) %all-to-all-start.4) | async-done | bytes 524320 | tf_op jit(solution)/shard_map/all_to_all | solution.py:83
  156.9 3.5 %scatter_custom_fusion = bf16[512,2048]{1,0:T(8,128)(2,1)S(1)} fusion(s32[256]{0:T(256)S(1)} %bitcast.142, bf16[256,2048]{1,0:T(8,128)(2,1)} %reshape.305, bf16[]{:T(256)} %constant.89.clone.1), kind=kCustom, calls=%fused_computation.50 | custom fusion | bytes 2097664 | tf_op jit(solution)/shard_map/scatter | solution.py:148
  160.4 53.4 %all_to_all.89 = bf16[8,64,2048]{2,1,0:T(8,128)(2,1)} all-to-all(bf16[8,64,2048]{2,1,0:T(8,128)(2,1)S(1)} %bitcast.127), channel_id=1, replica_groups=mesh['sp'=8,'dp'=4] {'sp'}, dimensions={0} | all-to-all | bytes 4194304 | tf_op jit(solution)/shard_map/all_to_all | solution.py:151
  213.8 9.5 %fusion.20 = f32[512,1792]{1,0:T(8,128)} fusion(bf16[512,2048]{1,0:T(8,128)(2,1)} %bitcast.41, bf16[1,2048,1792]{2,1,0:T(8,128)(2,1)} %param.25), kind=kOutput, calls=%fused_computation.30 | convolution fusion | flops 3758096384 | bytes 13107200 | tf_op jit(solution)/shard_map/dot_general | solution.py:154
  223.3 17.0 %fusion.24 = bf16[512,2048]{1,0:T(8,128)(2,1)} fusion(bf16[1,1792,2048]{2,1,0:T(8,128)(2,1)} %param.27, f32[512,1792]{1,0:T(8,128)} %fusion.20, bf16[512,2048]{1,0:T(8,128)(2,1)} %bitcast.41, bf16[1,2048,1792]{2,1,0:T(8,128)(2,1)} %param.26), kind=kOutput, calls=%fused_computation.33 | convolution fusion | flops 7522746368 | bytes 22544384 | tf_op jit(solution)/shard_map/dot_general | solution.py:157
  240.3 4.0 %all-to-all-start.6 = ((bf16[8,64,2048]{2,1,0:T(8,128)(2,1)}), bf16[8,64,2048]{2,1,0:T(8,128)(2,1)S(1)}, u32[]{:S(2)}, u32[]{:S(2)}) async-start(bf16[8,64,2048]{2,1,0:T(8,128)(2,1)} %bitcast.130), calls=%async_computation.6 | async-start | bytes 4194304 | tf_op jit(solution)/shard_map/all_to_all | solution.py:161
  245.7 46.2 %all-to-all-done.6 = bf16[8,64,2048]{2,1,0:T(8,128)(2,1)S(1)} async-done(((bf16[8,64,2048]{2,1,0:T(8,128)(2,1)}), bf16[8,64,2048]{2,1,0:T(8,128)(2,1)S(1)}, u32[]{:S(2)}, u32[]{:S(2)}) %all-to-all-start.6) | async-done | bytes 2097184 | tf_op jit(solution)/shard_map/all_to_all | solution.py:161
  291.9 1.4 gather_fusion
  293.3 1.3 reshape.290
  294.6 3.2 %multiply_reduce_fusion.2 = f32[128,2048]{1,0:T(8,128)S(1)} fusion(f32[128,2,2048]{2,1,0:T(2,128)S(1)} %reshape.290, f32[128,2]{1,0:T(8,128)S(1)} %copy.124), kind=kLoop, calls=%fused_computation.36 | loop fusion | flops 786432 | bytes 3146752 | tf_op jit(solution)/shard_map/reduce_sum | solution.py:167
  (86 shorter events, 23.9 us)
Async XLA Ops:
  9.4 9.1 %copy-start.3 = (bf16[1,128,16,128]{3,2,1,0:T(8,128)(2,1)S(1)}, bf16[1,128,16,128]{3,2,1,0:T(8,128)(2,1)}, u32[]{:S(2)}) copy-start(bf16[1,128,16,128]{3,2,1,0:T(8,128)(2,1)} %param.17) | copy-start | bytes 1572868
  9.4 9.5 %copy-start.8 = (f32[128]{0:T(128)S(1)}, f32[128]{0:T(128)}, u32[]{:S(2)}) copy-start(f32[128]{0:T(128)} %param.20) | copy-start | bytes 1540
  11.2 21.8 %all-to-all-start.1 = ((bf16[128,16,128]{2,0,1:T(8,128)(2,1)}), bf16[128,16,128]{2,0,1:T(8,128)(2,1)S(1)}, u32[]{:S(2)}, u32[]{:S(2)}) async-start(bf16[128,16,128]{2,0,1:T(8,128)(2,1)} %bitcast.12), calls=%async_computation.1 | async-start | bytes 1048576 | tf_op jit(solution)/shard_map/all_to_all | solution.py:114
  20.1 16.5 %copy-start.4 = (bf16[1,128,4,128]{3,2,1,0:T(4,128)(2,1)S(1)}, bf16[1,128,4,128]{3,2,1,0:T(4,128)(2,1)}, u32[]{:S(2)}) copy-start(bf16[1,128,4,128]{3,2,1,0:T(4,128)(2,1)} %param.19) | copy-start | bytes 393220
  33.0 18.3 %all-to-all-start = ((bf16[128,16,128]{2,0,1:T(8,128)(2,1)}), bf16[128,16,128]{2,0,1:T(8,128)(2,1)S(1)}, u32[]{:S(2)}, u32[]{:S(2)}) async-start(bf16[128,16,128]{2,0,1:T(8,128)(2,1)} %pad_maximum_fusion), calls=%async_computation | async-start | bytes 1048576 | tf_op jit(solution)/shard_map/all_to_all | solution.py:113
  52.2 18.3 %all-to-all-start.2 = ((bf16[128,16,128]{2,0,1:T(8,128)(2,1)}), bf16[128,16,128]{2,0,1:T(8,128)(2,1)S(1)}, u32[]{:S(2)}, u32[]{:S(2)}) async-start(bf16[128,16,128]{2,0,1:T(8,128)(2,1)} %bitcast.18), calls=%async_computation.2 | async-start | bytes 1048576 | tf_op jit(solution)/shard_map/all_to_all | solution.py:117
  55.8 57.9 %all-gather.5.cloned.1.call-start = ((), (), s32[]{:S(2)}) async-start(), calls=%async_computation.8 | async-start | bytes 2359296 | tf_op jit(solution)/shard_map/all_gather | solution.py:79
  56.6 80.3 %all-gather.3.cloned.1.call-start = ((), (), s32[]{:S(2)}) async-start(), calls=%async_computation.7 | async-start | bytes 2621440 | tf_op jit(solution)/shard_map/all_gather | solution.py:78
  106.2 1.4 copy-start.6
  141.1 12.3 %all-to-all-start.4 = ((bf16[4,128,512]{2,1,0:T(8,128)(2,1)}), bf16[4,128,512]{2,1,0:T(8,128)(2,1)S(1)}, u32[]{:S(2)}, u32[]{:S(2)}) async-start(bf16[4,128,512]{2,1,0:T(8,128)(2,1)} %fusion.29), calls=%async_computation.4 | async-start | bytes 1048576 | tf_op jit(solution)/shard_map/all_to_all | solution.py:83
  153.5 1.0 copy-start
  153.9 0.9 copy-start.5
  240.3 4.0 %copy-start.7 = (f32[1,128,2]{1,2,0:T(2,128)S(1)}, f32[1,128,2]{1,2,0:T(2,128)}, u32[]{:S(2)}) copy-start(f32[1,128,2]{1,2,0:T(2,128)} %param.29) | copy-start | bytes 3076
  240.3 51.6 %all-to-all-start.6 = ((bf16[8,64,2048]{2,1,0:T(8,128)(2,1)}), bf16[8,64,2048]{2,1,0:T(8,128)(2,1)S(1)}, u32[]{:S(2)}, u32[]{:S(2)}) async-start(bf16[8,64,2048]{2,1,0:T(8,128)(2,1)} %bitcast.130), calls=%async_computation.6 | async-start | bytes 4194304 | tf_op jit(solution)/shard_map/all_to_all | solution.py:161
  294.6 3.2 %copy-start.1 = (bf16[1,128,2048]{2,1,0:T(8,128)(2,1)S(1)}, bf16[1,128,2048]{2,1,0:T(8,128)(2,1)}, u32[]{:S(2)}) copy-start(bf16[1,128,2048]{2,1,0:T(8,128)(2,1)} %param.23) | copy-start | bytes 1572868
  294.6 3.2 %copy-start.2 = (f32[1,128,2048]{2,1,0:T(8,128)S(1)}, f32[1,128,2048]{2,1,0:T(8,128)}, u32[]{:S(2)}) copy-start(f32[1,128,2048]{2,1,0:T(8,128)} %copy.119) | copy-start | bytes 3145732
Sparse Core Ops, SparseCore 0:
  58.8 54.8 all-gather.4
  115.2 21.5 all-gather.2
where the time goes:
time: 306 us
  waiting for transfers between devices  123 us (40%)
  blocking collectives  81.4 us (27%)
  matrix products  35.4 us (12%)
  starting transfers between devices  22.2 us (7%)
  local copies, waits for them, and re-layouts  15.1 us (5%)
  other arithmetic  14.2 us (5%)
  between operations  13.8 us (5%)
    all_to_all x1, blocking collectives, on_device(): lax.all_to_all(buffer, 'sp', split_axis=0, concat_axis=0, tiled=True)  53.4 us
    all_to_all x1, waiting for transfers between devices, on_device(): lax.all_to_all(served, 'sp', split_axis=0, concat_axis=0, tiled=True)  46.2 us
    all_to_all x1, blocking collectives, on_device(): lax.all_to_all(by_heads, 'sp', split_axis=0, concat_axis=1, tiled=True)  28 us
    all_gather x1, waiting for transfers between devices, project_tokens(): all_rows = lax.all_gather(attended[None], 'dp', axis=0, tiled=True)  23.2 us
    dot_general x1, matrix products, on_device(): jnp.dot(hidden, expert_down[0], preferred_element_type=jnp.float32)  17 us
    all_to_all x1, waiting for transfers between devices, on_device(): lax.all_to_all(rot_query, 'sp', split_axis=1, concat_axis=0, tiled=True)  14.6 us
    all_to_all x1, waiting for transfers between devices, on_device(): lax.all_to_all(jnp.repeat(value_rows, group_size, axis=1), 'sp', split_ax...  13.7 us
    all_to_all x1, waiting for transfers between devices, on_device(): lax.all_to_all(jnp.repeat(rot_key, group_size, axis=1), 'sp', split_axis=...  11.4 us
  transfers between devices with their start and end apart: 7, of which 7 were waited for; matrix products, arithmetic and copies ran while one was open for 5% of the time, Pallas kernels for 0%

commit v1 on v0

v1 whole, which is shorter than its diff:
```python
import functools

import jax
import jax.numpy as jnp
from jax import lax
from jax.experimental import pallas as pl
from jax.experimental.pallas import tpu as pltpu
from jax.sharding import PartitionSpec as P

GRID_W = 64
EPS = 1e-06
THETA = 10000.0
MESH = pl.DeviceIdType.MESH
VMEM = pl.BlockSpec(memory_space=pltpu.VMEM)
ANY = pl.BlockSpec(memory_space=pl.ANY)
F32 = jnp.float32
BF16 = jnp.bfloat16


def rotation_tables(positions, head_width):
    quarter = head_width // 4
    inverse = THETA ** (-jnp.arange(quarter, dtype=F32) / quarter)
    grid_row = (positions // GRID_W).astype(F32)[:, None] * inverse[None, :]
    column = (positions % GRID_W).astype(F32)[:, None] * inverse[None, :]
    angles = jnp.concatenate([grid_row, grid_row, column, column], axis=-1)
    lane = jnp.arange(head_width) % (2 * quarter)
    sign = jnp.where(lane < quarter, -1.0, 1.0).astype(F32)
    return jnp.cos(angles), jnp.sin(angles) * sign[None, :]


def turn(rows, gain, cosine, sine):
    width = rows.shape[-1]
    quarter = width // 4
    a = rows.astype(F32)
    a = a * lax.rsqrt(jnp.mean(a * a, axis=-1, keepdims=True) + EPS) * gain
    lane = lax.broadcasted_iota(jnp.int32, a.shape, 1) % (2 * quarter)
    partner = jnp.where(
        lane < quarter, pltpu.roll(a, width - quarter, 1), pltpu.roll(a, quarter, 1)
    )
    return (a * cosine + partner * sine).astype(BF16)


def slot_choice(routes, slots, per_expert):
    rows = routes.shape[0]
    slot = lax.broadcasted_iota(jnp.int32, (rows, slots), 1)
    expert = slot // per_expert
    first = routes[:, 0:1] == expert
    second = routes[:, 1:2] == expert
    named = jnp.where(first | second, 1.0, 0.0).astype(BF16)
    earlier = lax.broadcasted_iota(jnp.int32, (rows, rows), 1) < lax.broadcasted_iota(
        jnp.int32, (rows, rows), 0
    )
    rank = jnp.dot(
        jnp.where(earlier, 1.0, 0.0).astype(BF16), named, preferred_element_type=F32
    )
    here = rank == (slot % per_expert).astype(F32)
    return (
        jnp.where(first & here, 1.0, 0.0).astype(BF16),
        jnp.where(second & here, 1.0, 0.0).astype(BF16),
    )


def attention_kernel(
    n,
    dp,
    slots,
    q_ref,
    k_ref,
    v_ref,
    qg_ref,
    kg_ref,
    cos_ref,
    sin_ref,
    w_ref,
    res_ref,
    ng_ref,
    routes_ref,
    mixed_ref,
    buf_ref,
    q_rot,
    kv,
    w_full,
    att,
    proj,
    back,
    kv_send,
    kv_recv,
    w_send,
    w_recv,
    y_send,
    y_recv,
    pair_send,
    pair_recv,
    fwd_send,
    fwd_recv,
    back_send,
    back_recv,
):
    me = lax.axis_index("sp")
    mine = lax.axis_index("dp")
    heads, rows, width = q_ref.shape
    kv_heads = k_ref.shape[0]
    group = heads // kv_heads
    model = heads * width
    ny = dp // 2
    core = mine % 2
    row_y = mine // 2
    partner = row_y * 2 + 1 - core

    barrier = pltpu.get_barrier_semaphore()
    for d in range(1, n):
        pl.semaphore_signal(
            barrier, inc=1, device_id={"sp": lax.rem(me + d, n)}, device_id_type=MESH
        )
    for d in range(1, dp):
        pl.semaphore_signal(
            barrier, inc=1, device_id={"dp": lax.rem(mine + d, dp)}, device_id_type=MESH
        )

    cosine = cos_ref[...]
    sine = sin_ref[...]
    my_rows = pl.ds(pl.multiple_of(me * rows, rows), rows)
    for g in range(kv_heads):
        kv[g, my_rows, :] = turn(k_ref[g], kg_ref[...], cosine, sine)
        kv[kv_heads + g, my_rows, :] = v_ref[g]
    pl.semaphore_wait(barrier, n - 1 + dp - 1)

    kv_copies = []
    w_rows = w_ref.shape[0]
    my_w = pl.ds(pl.multiple_of(me * w_rows, w_rows), w_rows)
    w_copies = []
    for d in range(1, n):
        copy = pltpu.make_async_remote_copy(
            src_ref=kv.at[:, my_rows, :],
            dst_ref=kv.at[:, my_rows, :],
            send_sem=kv_send.at[d],
            recv_sem=kv_recv.at[d],
            device_id={"sp": lax.rem(me + d, n)},
            device_id_type=MESH,
        )
        copy.start()
        kv_copies.append(copy)
    for d in range(1, n):
        copy = pltpu.make_async_remote_copy(
            src_ref=w_ref,
            dst_ref=w_full.at[my_w],
            send_sem=w_send.at[d],
            recv_sem=w_recv.at[d],
            device_id={"sp": lax.rem(me + d, n)},
            device_id_type=MESH,
        )
        copy.start()
        w_copies.append(copy)
    w_full[my_w] = w_ref[...]

    def turn_head(h, carry):
        q_rot[h] = turn(q_ref[h], qg_ref[...], cosine, sine)
        return carry

    lax.fori_loop(0, heads, turn_head, 0)
    for copy in kv_copies:
        copy.wait()

    per_step = 2
    scale = width ** (-0.5)
    pair_copies = []
    y_copies = {}
    for g in range(kv_heads):

        def some_heads(i, carry):
            first = g * group + i * per_step
            query = q_rot[pl.ds(first, per_step)].reshape(per_step * rows, width)
            scores = (
                lax.dot_general(
                    query, kv[g], (((1,), (1,)), ((), ())), preferred_element_type=F32
                )
                * scale
            )
            exponent = jnp.exp(scores - jnp.max(scores, axis=-1, keepdims=True))
            weights = (exponent / jnp.sum(exponent, axis=-1, keepdims=True)).astype(BF16)
            out = jnp.dot(weights, kv[kv_heads + g], preferred_element_type=F32).astype(BF16)
            for j in range(per_step):
                cols = pl.ds(pl.multiple_of((first + j) * width, width), width)
                att[mine, :, cols] = out[j * rows : (j + 1) * rows]
            return carry

        lax.fori_loop(0, group // per_step, some_heads, 0)
        cols = slice(g * group * width, (g + 1) * group * width)
        for j in range(1, ny):
            copy = pltpu.make_async_remote_copy(
                src_ref=att.at[mine, :, cols],
                dst_ref=att.at[mine, :, cols],
                send_sem=y_send.at[j, g],
                recv_sem=y_recv.at[j, g],
                device_id={"dp": lax.rem(row_y + j, ny) * 2 + core},
                device_id_type=MESH,
            )
            copy.start()
            y_copies[j, g] = copy
        copy = pltpu.make_async_remote_copy(
            src_ref=att.at[mine, :, cols],
            dst_ref=att.at[mine, :, cols],
            send_sem=pair_send.at[g],
            recv_sem=pair_recv.at[g],
            device_id={"dp": partner},
            device_id_type=MESH,
        )
        copy.start()
        pair_copies.append(copy)

    fwd_copies = {}

    def forward(j):
        source = lax.rem(row_y + ny - j, ny) * 2 + core
        for g in range(kv_heads):
            cols = slice(g * group * width, (g + 1) * group * width)
            y_copies[j, g].wait_recv()
            copy = pltpu.make_async_remote_copy(
                src_ref=att.at[source, :, cols],
                dst_ref=att.at[source, :, cols],
                send_sem=fwd_send.at[j, g],
                recv_sem=fwd_recv.at[j, g],
                device_id={"dp": partner},
                device_id_type=MESH,
            )
            copy.start()
            fwd_copies[j, g] = copy
        return source

    for copy in w_copies:
        copy.wait()

    def project(seq):
        return jnp.dot(att[seq], w_full[...], preferred_element_type=F32).astype(BF16)

    back_copies = []

    def send_back(seq, index):
        proj[index] = project(seq)
        copy = pltpu.make_async_remote_copy(
            src_ref=proj.at[index],
            dst_ref=back.at[mine],
            send_sem=back_send.at[index],
            recv_sem=back_recv.at[index],
            device_id={"dp": seq},
            device_id_type=MESH,
        )
        copy.start()
        back_copies.append(copy)

    index = 1
    back[mine] = project(mine)
    for copy in pair_copies:
        copy.wait_recv()
    send_back(partner, index)
    index += 1
    for j in range(1, ny):
        source = forward(j)
        send_back(source, index)
        index += 1
        for g in range(kv_heads):
            fwd_copies[j, g].wait_recv()
        send_back(lax.rem(row_y + ny - j, ny) * 2 + 1 - core, index)
        index += 1

    first_choice, second_choice = slot_choice(routes_ref[...], slots, slots // n)
    choice = first_choice + second_choice
    for copy in pair_copies:
        copy.wait_send()
    for j in range(1, ny):
        for g in range(kv_heads):
            y_copies[j, g].wait_send()
            fwd_copies[j, g].wait_send()
    for copy in back_copies:
        copy.wait()
    block = w_ref.shape[1]
    square = jnp.zeros((rows, 1), F32)
    for s in range(dp):
        cols = slice(s * block, (s + 1) * block)
        part = res_ref[:, cols].astype(F32) + back[s].astype(F32)
        mixed_ref[:, cols] = part
        square = square + jnp.sum(part * part, axis=-1, keepdims=True)
    factor = lax.rsqrt(square / model + EPS)
    for s in range(dp):
        cols = slice(s * block, (s + 1) * block)
        normed = (mixed_ref[:, cols] * factor * ng_ref[:, cols]).astype(BF16)
        buf_ref[:, cols] = lax.dot_general(
            choice, normed, (((0,), (0,)), ((), ())), preferred_element_type=F32
        ).astype(BF16)


def expert_kernel(
    n,
    groups,
    buf_ref,
    gate_hbm,
    up_hbm,
    down_hbm,
    mixed_ref,
    routes_ref,
    rw_ref,
    out_ref,
    gate,
    up,
    down,
    recv,
    hidden,
    res,
    ret,
    load_sem,
    go_send,
    go_recv,
    ret_send,
    ret_recv,
):
    me = lax.axis_index("sp")
    slots, model = buf_ref.shape
    per = slots // n
    ff = gate.shape[1]
    loads = [
        pltpu.make_async_copy(src.at[0], dst, load_sem.at[i])
        for i, (src, dst) in enumerate(((gate_hbm, gate), (up_hbm, up), (down_hbm, down)))
    ]
    barrier = pltpu.get_barrier_semaphore()
    for d in range(1, n):
        pl.semaphore_signal(
            barrier, inc=1, device_id={"sp": lax.rem(me + d, n)}, device_id_type=MESH
        )
    for load in loads:
        load.start()
    pl.semaphore_wait(barrier, n - 1)

    def rows_of(block):
        return pl.ds(pl.multiple_of(block * per, per), per)

    go = [None]
    for d in range(1, n):
        target = lax.rem(me + d, n)
        copy = pltpu.make_async_remote_copy(
            src_ref=buf_ref.at[rows_of(target)],
            dst_ref=recv.at[pl.ds(d * per, per)],
            send_sem=go_send.at[d],
            recv_sem=go_recv.at[d],
            device_id={"sp": target},
            device_id_type=MESH,
        )
        copy.start()
        go.append(copy)
    recv[0:per] = buf_ref[rows_of(me)]
    first_choice, second_choice = slot_choice(routes_ref[...], slots, per)

    share = n // groups
    tile = 256
    back = [None]
    for c in range(groups):
        for d in range(c * share, (c + 1) * share):
            if d > 0:
                go[d].wait_recv()
        lines = slice(c * share * per, (c + 1) * share * per)
        if c == 0:
            loads[0].wait()
            loads[1].wait()

        def up_tile(t, carry):
            cols = pl.ds(pl.multiple_of(t * tile, tile), tile)
            x = recv[lines]
            gate_part = jnp.dot(x, gate[:, cols], preferred_element_type=F32)
            up_part = jnp.dot(x, up[:, cols], preferred_element_type=F32)
            hidden[:, cols] = (gate_part / (1.0 + jnp.exp(-gate_part)) * up_part).astype(BF16)
            return carry

        lax.fori_loop(0, ff // tile, up_tile, 0)
        if c == 0:
            loads[2].wait()

        def down_tile(t, carry):
            cols = pl.ds(pl.multiple_of(t * tile, tile), tile)
            res[lines, cols] = jnp.dot(
                hidden[...], down[:, cols], preferred_element_type=F32
            ).astype(BF16)
            return carry

        lax.fori_loop(0, model // tile, down_tile, 0)
        for d in range(c * share, (c + 1) * share):
            if d == 0:
                ret[rows_of(me)] = res[0:per]
                continue
            copy = pltpu.make_async_remote_copy(
                src_ref=res.at[pl.ds(d * per, per)],
                dst_ref=ret.at[rows_of(me)],
                send_sem=ret_send.at[d],
                recv_sem=ret_recv.at[d],
                device_id={"sp": lax.rem(me + n - d, n)},
                device_id_type=MESH,
            )
            copy.start()
            back.append(copy)
    for d in range(1, n):
        go[d].wait_send()
        back[d].wait()
    for t in range(model // 512):
        cols = slice(t * 512, (t + 1) * 512)
        table = ret[:, cols]
        first = jnp.dot(first_choice, table, preferred_element_type=F32)
        second = jnp.dot(second_choice, table, preferred_element_type=F32)
        out_ref[:, cols] = (
            mixed_ref[:, cols] + (first * rw_ref[:, 0:1] + second * rw_ref[:, 1:2])
        ).astype(BF16)


def on_device(
    n,
    dp,
    queries,
    key_rows,
    values,
    query_gain,
    key_gain,
    out_weight,
    residual,
    norm_gain,
    expert_gate,
    expert_up,
    expert_down,
    routes,
    route_weight,
):
    _, rows, heads, width = queries.shape
    kv_heads = key_rows.shape[2]
    model = heads * width
    length = rows * n
    experts = expert_gate.shape[0] * n
    slots = experts * 2 * max(2, 4 * (rows // 2) // experts)
    positions = lax.axis_index("sp") * rows + jnp.arange(rows, dtype=jnp.int32)
    cosine, sine = rotation_tables(positions, width)
    w_rows, w_cols = out_weight.shape
    dma = pltpu.SemaphoreType.DMA
    ny = dp // 2
    mixed, buffer = pl.pallas_call(
        functools.partial(attention_kernel, n, dp, slots),
        out_shape=(
            jax.ShapeDtypeStruct((rows, model), F32),
            jax.ShapeDtypeStruct((slots, model), BF16),
        ),
        in_specs=[VMEM] * 11,
        out_specs=(VMEM, VMEM),
        scratch_shapes=[
            pltpu.VMEM((heads, rows, width), BF16),
            pltpu.VMEM((2 * kv_heads, length, width), BF16),
            pltpu.VMEM((w_rows * n, w_cols), BF16),
            pltpu.VMEM((dp, rows, model), BF16),
            pltpu.VMEM((dp, rows, w_cols), BF16),
            pltpu.VMEM((dp, rows, w_cols), BF16),
            dma((n,)),
            dma((n,)),
            dma((n,)),
            dma((n,)),
            dma((ny, kv_heads)),
            dma((ny, kv_heads)),
            dma((kv_heads,)),
            dma((kv_heads,)),
            dma((ny, kv_heads)),
            dma((ny, kv_heads)),
            dma((dp,)),
            dma((dp,)),
        ],
        compiler_params=pltpu.CompilerParams(
            collective_id=0, has_side_effects=True, vmem_limit_bytes=40 * 1024 * 1024
        ),
        name="attention",
    )(
        queries[0].transpose(1, 0, 2),
        key_rows[0].transpose(1, 0, 2),
        values[0].transpose(1, 0, 2),
        query_gain[None],
        key_gain[None],
        cosine,
        sine,
        out_weight,
        residual[0],
        norm_gain[None],
        routes[0],
    )
    ff = expert_gate.shape[2]
    groups = 2
    result = pl.pallas_call(
        functools.partial(expert_kernel, n, groups),
        out_shape=jax.ShapeDtypeStruct((rows, model), BF16),
        in_specs=[VMEM, ANY, ANY, ANY, VMEM, VMEM, VMEM],
        out_specs=VMEM,
        scratch_shapes=[
            pltpu.VMEM((model, ff), BF16),
            pltpu.VMEM((model, ff), BF16),
            pltpu.VMEM((ff, model), BF16),
            pltpu.VMEM((slots, model), BF16),
            pltpu.VMEM((slots // groups, ff), BF16),
            pltpu.VMEM((slots, model), BF16),
            pltpu.VMEM((slots, model), BF16),
            dma((3,)),
            dma((n,)),
            dma((n,)),
            dma((n,)),
            dma((n,)),
        ],
        compiler_params=pltpu.CompilerParams(
            collective_id=1, has_side_effects=True, vmem_limit_bytes=56 * 1024 * 1024
        ),
        name="experts",
    )(
        buffer,
        expert_gate,
        expert_up,
        expert_down,
        mixed,
        routes[0],
        route_weight[0],
    )
    return result[None]


def solution(mesh):
    in_specs = (
        P("dp", "sp", None, None),
        P("dp", "sp", None, None),
        P("dp", "sp", None, None),
        P(),
        P(),
        P("sp", "dp"),
        P("dp", "sp", None),
        P(),
        P("sp", None, None),
        P("sp", None, None),
        P("sp", None, None),
        P("dp", "sp", None),
        P("dp", "sp", None),
    )
    out_specs = P("dp", "sp", None)
    return jax.shard_map(
        functools.partial(on_device, mesh.shape["sp"], mesh.shape["dp"]),
        mesh=mesh,
        in_specs=in_specs,
        out_specs=out_specs,
        check_vma=False,
    )
```

time: 306 us -> 236 us (0.77)
  Pallas kernels: 0 us -> 222 us
  waiting for transfers between devices: 123 us -> 0 us
  blocking collectives: 81.4 us -> 0 us
  matrix products: 35.4 us -> 0 us
  starting transfers between devices: 22.2 us -> 0 us
  other arithmetic: 14.2 us -> 0.47 us
  between operations: 13.8 us -> 0.08 us
    pallas_call x0 -> x2, Pallas kernels: none -> 222 us  [the longest x1 131 us: on_device(): pl.pallas_call(functools.partial(expert_kernel, n, groups), out_shape=jax...]
    all_to_all x5 -> x0, waiting for transfers between devices: 94.5 us -> none  [the longest x1 46.2 us: on_device(): lax.all_to_all(served, 'sp', split_axis=0, concat_axis=0, tiled=True)]
    all_to_all x2 -> x0, blocking collectives: 81.4 us -> none  [the longest x1 53.4 us: on_device(): lax.all_to_all(buffer, 'sp', split_axis=0, concat_axis=0, tiled=True)]
    dot_general x11 -> x0, matrix products: 35.4 us -> none  [the longest x1 17 us: on_device(): jnp.dot(hidden, expert_down[0], preferred_element_type=jnp.float32)]
    all_gather x2 -> x0, waiting for transfers between devices: 28.3 us -> none  [the longest x1 23.2 us: project_tokens(): all_rows = lax.all_gather(attended[None], 'dp', axis=0, tiled=True)]
    all_to_all x5 -> x0, starting transfers between devices: 22.2 us -> none  [the longest x1 7.28 us: on_device(): lax.all_to_all(jnp.repeat(rot_key, group_size, axis=1), 'sp', split_axis=...]
    unnamed x19 -> x20, local copies, waits for them, and re-layouts: 0.51 us -> 11.6 us
    reduce_sum x9 -> x0, other arithmetic: 7.18 us -> none  [the longest x1 3.18 us: on_device(): result = mixed_sum + jnp.sum(picked * route_weight[0][..., None], axis=1)]
  transfers between devices with their start and end apart: 7 -> 0, of which waited for: 7 -> 0; matrix products, arithmetic and copies ran while one was open for 5% -> 0% of each run, Pallas kernels for 0% -> 0%
where the time goes in v1:
time: 236 us; the launch traced here: 235 us
  Pallas kernels  222 us (94%)
  local copies, waits for them, and re-layouts  12.6 us (5%)
    pallas_call x1, Pallas kernels, on_device(): pl.pallas_call(functools.partial(expert_kernel, n, groups), out_shape=jax...  131 us
    pallas_call x1, Pallas kernels, on_device(): pl.pallas_call(functools.partial(attention_kernel, n, dp, slots), out_sha...  91 us
    unnamed x20, local copies, waits for them, and re-layouts  11.6 us

profile of v1, /device:TPU:0, one launch (start us, length us, event | category | flops | bytes accessed | tf_op | source)
XLA Modules:
  0.0 235.3 jit_solution(10555350160265042719)
XLA Ops:
  0.0 0.1 broadcast_multiply_fusion.1
  0.1 0.3 sine_multiply_fusion
  0.5 1.0 copy_bitcast_fusion.1
  1.5 0.8 copy.17
  2.3 0.0 copy-start.2
  2.3 1.2 copy.22
  3.5 0.0 copy-start.3
  3.5 1.0 copy-done.3
  4.6 0.0 copy-start.4
  4.6 0.9 copy-done.4
  5.5 0.7 copy-done.5
  6.2 0.0 copy-start.6
  6.2 0.7 copy-done.6
  6.9 0.0 copy-start.7
  6.9 0.7 copy-done.7
  7.5 91.0 %attention.1 = (f32[128,2048]{1,0:T(8,128)S(1)}, bf16[512,2048]{1,0:T(8,128)(2,1)S(1)}) custom-call(bf16[16,128,128]{2,1,0:T(8,128)(2,1)S(1)} %bitcast.20, bf16[4,128,128]{2,1,0:T(8,128)(2,1)S(1)} %get-tuple-element.16.k_ref, bf16[4,128,128]{2,1,0:T(8,128)(2,1)S(1)} %get-tuple-element.15.v_ref, f32[1,128]{1,0:T(1,128)S(1)} %bitcast.25, ...), custom_call_target="tpu_custom_call" | custom-call | tf_op jit(solution)/shard_map/attention/pallas_call | solution.py:439
  98.5 0.0 copy-start
  98.6 1.3 copy-done
  99.9 0.0 copy-start.1
  99.9 1.0 copy-done.1
  100.8 1.4 copy.18
  102.2 0.0 copy-done.2
  102.2 131.1 %experts.1 = bf16[128,2048]{1,0:T(8,128)(2,1)} custom-call(bf16[512,2048]{1,0:T(8,128)(2,1)} %copy-done, bf16[1,2048,1792]{2,1,0:T(8,128)(2,1)} %gate_hbm.1, bf16[1,2048,1792]{2,1,0:T(8,128)(2,1)} %up_hbm.1, bf16[1,1792,2048]{2,1,0:T(8,128)(2,1)} %down_hbm.1, f32[128,2048]{1,0:T(8,128)} %copy-done.1, s32[128,2]{1,0:T(8,128)} %bitcast.22, f32[128,2]{1,0:T(8,128)} %bitcast.28), custom_call_target="tpu_custom_call" | custom-call | tf_op jit(solution)/shard_map/experts/pallas_call | solution.py:486
  233.4 1.9 copy.24
  (4 shorter events, 0.0 us)
Async XLA Ops:
  2.3 100.0 %copy-start.2 = (s32[1,128,2]{2,1,0:T(8,128)}, s32[1,128,2]{2,1,0:T(8,128)S(1)}, u32[]{:S(2)}) copy-start(s32[1,128,2]{2,1,0:T(8,128)S(1)} %copy.17) | copy-start | bytes 3076
  3.5 1.0 copy-start.3
  4.6 0.9 copy-start.4
  5.5 0.7 copy-start.5
  6.2 0.7 copy-start.6
  6.9 0.7 copy-start.7
  98.5 1.3 copy-start
  99.9 1.0 copy-start.1

commit v2 on v1

--- a/solution.py
+++ b/solution.py
@@ -40,12 +40,109 @@
     return (a * cosine + partner * sine).astype(BF16)
 
 
-def slot_choice(routes, slots, per_expert):
-    rows = routes.shape[0]
+class Spread:
+    def __init__(self, n, block, send, recv, z_first):
+        self.width = max(x for x in range(1, n + 1) if n % x == 0 and x * x <= n)
+        self.depth = n // self.width
+        self.block, self.send, self.recv, self.z_first = block, send, recv, z_first
+        me = lax.axis_index("sp")
+        self.z, self.x = me // self.width, me % self.width
+        self.ends = []
+
+    def copy(self, source, way, target):
+        return pltpu.make_async_remote_copy(
+            src_ref=self.block(source),
+            dst_ref=self.block(source),
+            send_sem=self.send.at[source, way],
+            recv_sem=self.recv.at[source],
+            device_id={"sp": target},
+            device_id_type=MESH,
+        )
+
+    def at(self, z, x):
+        return z * self.width + x
+
+    def start(self, condition, source, way, target):
+        @pl.when(condition)
+        def _():
+            self.copy(source, way, target).start()
+
+        self.ends.append((condition, source, way, target))
+
+    def up(self, condition, source):
+        ok = condition & (self.z < self.depth - 1)
+        self.start(ok, source, 0, self.at(self.z + 1, self.x))
+
+    def down(self, condition, source):
+        ok = condition & (self.z > 0)
+        self.start(ok, source, 1, self.at(self.z - 1, self.x))
+
+    def across(self, condition, source):
+        for k in range(1, self.width):
+            self.start(condition, source, 1 + k, self.at(self.z, (self.x + k) % self.width))
+
+    def arrive(self, condition, source):
+        @pl.when(condition)
+        def _():
+            self.copy(source, 0, source).wait_recv()
+
+    def columns(self):
+        if self.z_first:
+            return [self.x]
+        return [(self.x + k) % self.width for k in range(self.width)]
+
+    def begin(self):
+        own = self.at(self.z, self.x)
+        always = self.z >= 0
+        if not self.z_first:
+            self.across(always, own)
+        self.up(always, own)
+        self.down(always, own)
+        if self.z_first:
+            self.across(always, own)
+
+    def second(self):
+        always = self.z >= 0
+        for x in self.columns()[1:]:
+            source = self.at(self.z, x)
+            self.arrive(always, source)
+            self.up(always, source)
+            self.down(always, source)
+
+    def step(self, t):
+        for x in self.columns():
+            below, above = self.z - t >= 0, self.z + t < self.depth
+            source = self.at(self.z - t, x)
+            self.arrive(below, source)
+            self.up(below, source)
+            if self.z_first:
+                self.across(below, source)
+            source = self.at(self.z + t, x)
+            self.arrive(above, source)
+            self.down(above, source)
+            if self.z_first:
+                self.across(above, source)
+
+    def finish(self):
+        always = self.z >= 0
+        for z in range(self.depth):
+            for k in range(1, self.width):
+                self.arrive(always, self.at(z, (self.x + k) % self.width))
+
+    def drain(self):
+        for condition, source, way, target in self.ends:
+
+            @pl.when(condition)
+            def _():
+                self.copy(source, way, target).wait_send()
+
+
+def slot_choice(table, base, slots, capacity):
+    rows = table.shape[0]
     slot = lax.broadcasted_iota(jnp.int32, (rows, slots), 1)
-    expert = slot // per_expert
-    first = routes[:, 0:1] == expert
-    second = routes[:, 1:2] == expert
+    expert = (slot // capacity + base).astype(F32)
+    first = table[:, 0:1] == expert
+    second = table[:, 1:2] == expert
     named = jnp.where(first | second, 1.0, 0.0).astype(BF16)
     earlier = lax.broadcasted_iota(jnp.int32, (rows, rows), 1) < lax.broadcasted_iota(
         jnp.int32, (rows, rows), 0
@@ -53,7 +150,7 @@
     rank = jnp.dot(
         jnp.where(earlier, 1.0, 0.0).astype(BF16), named, preferred_element_type=F32
     )
-    here = rank == (slot % per_expert).astype(F32)
+    here = rank == (slot % capacity).astype(F32)
     return (
         jnp.where(first & here, 1.0, 0.0).astype(BF16),
         jnp.where(second & here, 1.0, 0.0).astype(BF16),
@@ -63,7 +160,6 @@
 def attention_kernel(
     n,
     dp,
-    slots,
     q_ref,
     k_ref,
     v_ref,
@@ -74,19 +170,20 @@
     w_ref,
     res_ref,
     ng_ref,
-    routes_ref,
+    table_ref,
     mixed_ref,
-    buf_ref,
+    normed_ref,
+    other_ref,
     q_rot,
     kv,
     w_full,
     att,
     proj,
     back,
-    kv_send,
-    kv_recv,
-    w_send,
-    w_recv,
+    table,
+    x_send,
+    x_recv,
+    t_sem,
     y_send,
     y_recv,
     pair_send,
@@ -125,41 +222,55 @@
         kv[kv_heads + g, my_rows, :] = v_ref[g]
     pl.semaphore_wait(barrier, n - 1 + dp - 1)
 
-    kv_copies = []
     w_rows = w_ref.shape[0]
     my_w = pl.ds(pl.multiple_of(me * w_rows, w_rows), w_rows)
-    w_copies = []
-    for d in range(1, n):
-        copy = pltpu.make_async_remote_copy(
-            src_ref=kv.at[:, my_rows, :],
-            dst_ref=kv.at[:, my_rows, :],
-            send_sem=kv_send.at[d],
-            recv_sem=kv_recv.at[d],
-            device_id={"sp": lax.rem(me + d, n)},
-            device_id_type=MESH,
-        )
-        copy.start()
-        kv_copies.append(copy)
-    for d in range(1, n):
-        copy = pltpu.make_async_remote_copy(
-            src_ref=w_ref,
-            dst_ref=w_full.at[my_w],
-            send_sem=w_send.at[d],
-            recv_sem=w_recv.at[d],
-            device_id={"sp": lax.rem(me + d, n)},
-            device_id_type=MESH,
-        )
-        copy.start()
-        w_copies.append(copy)
     w_full[my_w] = w_ref[...]
+
+    def key_block(s):
+        return kv.at[pl.ds(0, kv_heads), pl.ds(pl.multiple_of(s * rows, rows), rows), :]
+
+    def value_block(s):
+        return kv.at[pl.ds(kv_heads, kv_heads), pl.ds(pl.multiple_of(s * rows, rows), rows), :]
+
+    def weight_block(part):
+        size = w_rows // 2
+        return lambda s: w_full.at[
+            pl.ds(pl.multiple_of(s * w_rows + part * size, size), size)
+        ]
+
+    attention_gather = (
+        Spread(n, value_block, x_send.at[0], x_recv.at[0], False),
+        Spread(n, key_block, x_send.at[1], x_recv.at[1], True),
+    )
+    weight_gather = (
+        Spread(n, weight_block(1), x_send.at[2], x_recv.at[2], False),
+        Spread(n, weight_block(0), x_send.at[3], x_recv.at[3], True),
+    )
+    table_copy = pltpu.make_async_remote_copy(
+        src_ref=table_ref,
+        dst_ref=table,
+        send_sem=t_sem.at[0],
+        recv_sem=t_sem.at[1],
+        device_id={"sp": lax.rem(me + n // 2, n)},
+        device_id_type=MESH,
+    )
+    table_copy.start()
+    for spread in attention_gather:
+        spread.begin()
 
     def turn_head(h, carry):
         q_rot[h] = turn(q_ref[h], qg_ref[...], cosine, sine)
         return carry
 
     lax.fori_loop(0, heads, turn_head, 0)
-    for copy in kv_copies:
-        copy.wait()
+    attention_gather[0].second()
+    steps = attention_gather[0].depth
+    for t in range(1, steps):
+        for spread in attention_gather:
+            spread.step(t)
+    for spread in weight_gather:
+        spread.begin()
+    attention_gather[1].finish()
 
     per_step = 2
     scale = width ** (-0.5)
@@ -207,7 +318,13 @@
         )
         copy.start()
         pair_copies.append(copy)
-
+        if g == 0:
+            weight_gather[0].second()
+
+    for t in range(1, steps):
+        for spread in weight_gather:
+            spread.step(t)
+    weight_gather[1].finish()
     fwd_copies = {}
 
     def forward(j):
@@ -227,9 +344,6 @@
             fwd_copies[j, g] = copy
         return source
 
-    for copy in w_copies:
-        copy.wait()
-
     def project(seq):
         return jnp.dot(att[seq], w_full[...], preferred_element_type=F32).astype(BF16)
 
@@ -263,8 +377,10 @@
         send_back(lax.rem(row_y + ny - j, ny) * 2 + 1 - core, index)
         index += 1
 
-    first_choice, second_choice = slot_choice(routes_ref[...], slots, slots // n)
-    choice = first_choice + second_choice
+    for spread in attention_gather + weight_gather:
+        spread.drain()
+    table_copy.wait()
+    other_ref[...] = table[...]
     for copy in pair_copies:
         copy.wait_send()
     for j in range(1, ny):
@@ -283,129 +399,208 @@
     factor = lax.rsqrt(square / model + EPS)
     for s in range(dp):
         cols = slice(s * block, (s + 1) * block)
-        normed = (mixed_ref[:, cols] * factor * ng_ref[:, cols]).astype(BF16)
-        buf_ref[:, cols] = lax.dot_general(
-            choice, normed, (((0,), (0,)), ((), ())), preferred_element_type=F32
-        ).astype(BF16)
+        normed_ref[:, cols] = (mixed_ref[:, cols] * factor * ng_ref[:, cols]).astype(BF16)
 
 
 def expert_kernel(
     n,
-    groups,
-    buf_ref,
+    capacity,
+    normed_ref,
+    mixed_ref,
+    own_ref,
+    other_ref,
     gate_hbm,
     up_hbm,
     down_hbm,
-    mixed_ref,
-    routes_ref,
-    rw_ref,
     out_ref,
     gate,
     up,
     down,
+    relay,
+    sent,
     recv,
     hidden,
     res,
     ret,
+    part,
+    home,
+    hold,
     load_sem,
+    relay_sem,
+    home_sem,
     go_send,
     go_recv,
     ret_send,
     ret_recv,
 ):
     me = lax.axis_index("sp")
-    slots, model = buf_ref.shape
-    per = slots // n
+    half = n // 2
+    base = me // half * half
+    mine = me % half
+    partner = lax.rem(me + half, n)
+    rows, model = normed_ref.shape
+    few = rows // 2
+    slots = half * capacity
     ff = gate.shape[1]
     loads = [
         pltpu.make_async_copy(src.at[0], dst, load_sem.at[i])
         for i, (src, dst) in enumerate(((gate_hbm, gate), (up_hbm, up), (down_hbm, down)))
     ]
+
+    def peer(k):
+        return base + lax.rem(mine + k, half)
+
     barrier = pltpu.get_barrier_semaphore()
-    for d in range(1, n):
-        pl.semaphore_signal(
-            barrier, inc=1, device_id={"sp": lax.rem(me + d, n)}, device_id_type=MESH
-        )
+    for target in [partner] + [peer(k) for k in range(1, half)]:
+        pl.semaphore_signal(barrier, inc=1, device_id={"sp": target}, device_id_type=MESH)
     for load in loads:
         load.start()
-    pl.semaphore_wait(barrier, n - 1)
-
-    def rows_of(block):
-        return pl.ds(pl.multiple_of(block * per, per), per)
-
-    go = [None]
-    for d in range(1, n):
-        target = lax.rem(me + d, n)
+    pl.semaphore_wait(barrier, half)
+
+    relays = []
+    for b in range(2):
         copy = pltpu.make_async_remote_copy(
-            src_ref=buf_ref.at[rows_of(target)],
-            dst_ref=recv.at[pl.ds(d * per, per)],
-            send_sem=go_send.at[d],
-            recv_sem=go_recv.at[d],
-            device_id={"sp": target},
+            src_ref=normed_ref.at[pl.ds(b * few, few)],
+            dst_ref=relay.at[b],
+            send_sem=relay_sem.at[0, b],
+            recv_sem=relay_sem.at[1, b],
+            device_id={"sp": partner},
             device_id_type=MESH,
         )
         copy.start()
-        go.append(copy)
-    recv[0:per] = buf_ref[rows_of(me)]
-    first_choice, second_choice = slot_choice(routes_ref[...], slots, per)
-
-    share = n // groups
+        relays.append(copy)
+
+    def block(index):
+        return pl.ds(pl.multiple_of(index * capacity, capacity), capacity)
+
+    go, back, homes = {}, {}, []
+
+    def choices(r):
+        table = own_ref if r < 2 else other_ref
+        return slot_choice(table[(r % 2) * few : (r % 2 + 1) * few], base, slots, capacity)
+
+    def dispatch(r):
+        first, second = choices(r)
+        choice = first + second
+        lines = normed_ref[(r % 2) * few : (r % 2 + 1) * few] if r < 2 else relay[r % 2]
+        for t in range(model // 512):
+            cols = slice(t * 512, (t + 1) * 512)
+            sent[r, :, cols] = lax.dot_general(
+                choice, lines[:, cols], (((0,), (0,)), ((), ())), preferred_element_type=F32
+            ).astype(BF16)
+        recv[r, block(mine)] = sent[r, block(mine)]
+        for k in range(1, half):
+            copy = pltpu.make_async_remote_copy(
+                src_ref=sent.at[r, block(lax.rem(mine + k, half))],
+                dst_ref=recv.at[r, block(mine)],
+                send_sem=go_send.at[r, k],
+                recv_sem=go_recv.at[r, k],
+                device_id={"sp": peer(k)},
+                device_id_type=MESH,
+            )
+            copy.start()
+            go[r, k] = copy
+
     tile = 256
-    back = [None]
-    for c in range(groups):
-        for d in range(c * share, (c + 1) * share):
-            if d > 0:
-                go[d].wait_recv()
-        lines = slice(c * share * per, (c + 1) * share * per)
-        if c == 0:
-            loads[0].wait()
-            loads[1].wait()
+
+    def serve(r):
+        for k in range(1, half):
+            go[r, k].wait_recv()
 
         def up_tile(t, carry):
             cols = pl.ds(pl.multiple_of(t * tile, tile), tile)
-            x = recv[lines]
-            gate_part = jnp.dot(x, gate[:, cols], preferred_element_type=F32)
-            up_part = jnp.dot(x, up[:, cols], preferred_element_type=F32)
+            gate_part = jnp.dot(recv[r], gate[:, cols], preferred_element_type=F32)
+            up_part = jnp.dot(recv[r], up[:, cols], preferred_element_type=F32)
             hidden[:, cols] = (gate_part / (1.0 + jnp.exp(-gate_part)) * up_part).astype(BF16)
             return carry
 
         lax.fori_loop(0, ff // tile, up_tile, 0)
-        if c == 0:
+        if r == 0:
             loads[2].wait()
 
         def down_tile(t, carry):
             cols = pl.ds(pl.multiple_of(t * tile, tile), tile)
-            res[lines, cols] = jnp.dot(
+            res[r, :, cols] = jnp.dot(
                 hidden[...], down[:, cols], preferred_element_type=F32
             ).astype(BF16)
             return carry
 
         lax.fori_loop(0, model // tile, down_tile, 0)
-        for d in range(c * share, (c + 1) * share):
-            if d == 0:
-                ret[rows_of(me)] = res[0:per]
-                continue
+        ret[r, block(mine)] = res[r, block(mine)]
+        for k in range(1, half):
             copy = pltpu.make_async_remote_copy(
-                src_ref=res.at[pl.ds(d * per, per)],
-                dst_ref=ret.at[rows_of(me)],
-                send_sem=ret_send.at[d],
-                recv_sem=ret_recv.at[d],
-                device_id={"sp": lax.rem(me + n - d, n)},
+                src_ref=res.at[r, block(lax.rem(mine + k, half))],
+                dst_ref=ret.at[r, block(mine)],
+                send_sem=ret_send.at[r, k],
+                recv_sem=ret_recv.at[r, k],
+                device_id={"sp": peer(k)},
                 device_id_type=MESH,
             )
             copy.start()
-            back.append(copy)
-    for d in range(1, n):
-        go[d].wait_send()
-        back[d].wait()
-    for t in range(model // 512):
-        cols = slice(t * 512, (t + 1) * 512)
-        table = ret[:, cols]
-        first = jnp.dot(first_choice, table, preferred_element_type=F32)
-        second = jnp.dot(second_choice, table, preferred_element_type=F32)
-        out_ref[:, cols] = (
-            mixed_ref[:, cols] + (first * rw_ref[:, 0:1] + second * rw_ref[:, 1:2])
-        ).astype(BF16)
+            back[r, k] = copy
+
+    def combine(r, store):
+        first, second = choices(r)
+        table = own_ref if r < 2 else other_ref
+        lines = slice((r % 2) * few, (r % 2 + 1) * few)
+        for k in range(1, half):
+            back[r, k].wait_recv()
+        for t in range(model // 512):
+            cols = slice(t * 512, (t + 1) * 512)
+            served = ret[r, :, cols]
+            store(
+                lines,
+                cols,
+                jnp.dot(first, served, preferred_element_type=F32) * table[lines, 2:3]
+                + jnp.dot(second, served, preferred_element_type=F32) * table[lines, 3:4],
+            )
+
+    def store_part(lines, cols, value):
+        part[lines, cols] = value.astype(BF16)
+
+    def send_home(b):
+        combine(2 + b, store_part)
+        copy = pltpu.make_async_remote_copy(
+            src_ref=part.at[pl.ds(b * few, few)],
+            dst_ref=home.at[b],
+            send_sem=home_sem.at[0, b],
+            recv_sem=home_sem.at[1, b],
+            device_id={"sp": partner},
+            device_id_type=MESH,
+        )
+        copy.start()
+        homes.append(copy)
+
+    def store_own(lines, cols, value):
+        hold[lines, cols] = mixed_ref[lines, cols] + value
+
+    dispatch(0)
+    dispatch(1)
+    loads[0].wait()
+    loads[1].wait()
+    serve(0)
+    relays[0].wait_recv()
+    dispatch(2)
+    serve(1)
+    relays[1].wait_recv()
+    dispatch(3)
+    serve(2)
+    serve(3)
+    send_home(0)
+    send_home(1)
+    combine(0, store_own)
+    combine(1, store_own)
+    for b in range(2):
+        homes[b].wait_recv()
+        lines = slice(b * few, (b + 1) * few)
+        out_ref[lines] = (hold[lines] + home[b].astype(F32)).astype(BF16)
+    for b in range(2):
+        relays[b].wait_send()
+        homes[b].wait_send()
+    for r in range(4):
+        for k in range(1, half):
+            go[r, k].wait_send()
+            back[r, k].wait_send()
 
 
 def on_device(
@@ -430,20 +625,25 @@
     model = heads * width
     length = rows * n
     experts = expert_gate.shape[0] * n
-    slots = experts * 2 * max(2, 4 * (rows // 2) // experts)
+    capacity = max(2, 4 * (rows // 2) // experts)
+    slots = n // 2 * capacity
+    table = jnp.concatenate([routes[0].astype(F32), route_weight[0]], axis=-1)
+    table = jnp.pad(table, ((0, 0), (0, width - table.shape[1])))
+    x_width = max(x for x in range(1, n + 1) if n % x == 0 and x * x <= n)
     positions = lax.axis_index("sp") * rows + jnp.arange(rows, dtype=jnp.int32)
     cosine, sine = rotation_tables(positions, width)
     w_rows, w_cols = out_weight.shape
     dma = pltpu.SemaphoreType.DMA
     ny = dp // 2
-    mixed, buffer = pl.pallas_call(
-        functools.partial(attention_kernel, n, dp, slots),
+    mixed, normed, other = pl.pallas_call(
+        functools.partial(attention_kernel, n, dp),
         out_shape=(
             jax.ShapeDtypeStruct((rows, model), F32),
-            jax.ShapeDtypeStruct((slots, model), BF16),
+            jax.ShapeDtypeStruct((rows, model), BF16),
+            jax.ShapeDtypeStruct(table.shape, F32),
         ),
         in_specs=[VMEM] * 11,
-        out_specs=(VMEM, VMEM),
+        out_specs=(VMEM, VMEM, VMEM),
         scratch_shapes=[
             pltpu.VMEM((heads, rows, width), BF16),
             pltpu.VMEM((2 * kv_heads, length, width), BF16),
@@ -451,10 +651,10 @@
             pltpu.VMEM((dp, rows, model), BF16),
             pltpu.VMEM((dp, rows, w_cols), BF16),
             pltpu.VMEM((dp, rows, w_cols), BF16),
-            dma((n,)),
-            dma((n,)),
-            dma((n,)),
-            dma((n,)),
+            pltpu.VMEM(table.shape, F32),
+            dma((4, n, 1 + x_width)),
+            dma((4, n)),
+            dma((2,)),
             dma((ny, kv_heads)),
             dma((ny, kv_heads)),
             dma((kv_heads,)),
@@ -479,42 +679,41 @@
         out_weight,
         residual[0],
         norm_gain[None],
-        routes[0],
+        table,
     )
     ff = expert_gate.shape[2]
-    groups = 2
+    few = rows // 2
     result = pl.pallas_call(
-        functools.partial(expert_kernel, n, groups),
+        functools.partial(expert_kernel, n, capacity),
         out_shape=jax.ShapeDtypeStruct((rows, model), BF16),
-        in_specs=[VMEM, ANY, ANY, ANY, VMEM, VMEM, VMEM],
+        in_specs=[VMEM, VMEM, VMEM, VMEM, ANY, ANY, ANY],
         out_specs=VMEM,
         scratch_shapes=[
             pltpu.VMEM((model, ff), BF16),
             pltpu.VMEM((model, ff), BF16),
             pltpu.VMEM((ff, model), BF16),
-            pltpu.VMEM((slots, model), BF16),
-            pltpu.VMEM((slots // groups, ff), BF16),
-            pltpu.VMEM((slots, model), BF16),
-            pltpu.VMEM((slots, model), BF16),
+            pltpu.VMEM((2, few, model), BF16),
+            pltpu.VMEM((4, slots, model), BF16),
+            pltpu.VMEM((4, slots, model), BF16),
+            pltpu.VMEM((slots, ff), BF16),
+            pltpu.VMEM((4, slots, model), BF16),
+            pltpu.VMEM((4, slots, model), BF16),
+            pltpu.VMEM((rows, model), BF16),
+            pltpu.VMEM((2, few, model), BF16),
+            pltpu.VMEM((rows, model), F32),
             dma((3,)),
-            dma((n,)),
-            dma((n,)),
-            dma((n,)),
-            dma((n,)),
+            dma((2, 2)),
+            dma((2, 2)),
+            dma((4, n)),
+            dma((4, n)),
+            dma((4, n)),
+            dma((4, n)),
         ],
         compiler_params=pltpu.CompilerParams(
             collective_id=1, has_side_effects=True, vmem_limit_bytes=56 * 1024 * 1024
         ),
         name="experts",
-    )(
-        buffer,
-        expert_gate,
-        expert_up,
-        expert_down,
-        mixed,
-        routes[0],
-        route_weight[0],
-    )
+    )(normed, mixed, table, other, expert_gate, expert_up, expert_down)
     return result[None]
 
 

time: 236 us -> 168 us (0.71)
  Pallas kernels: 222 us -> 155 us
    pallas_call x2, Pallas kernels: 222 us -> 155 us  [the longest x1 81.8 us: on_device(): pl.pallas_call(functools.partial(expert_kernel, n, capacity), out_shape=j...]
where the time goes in v2:
time: 168 us; the launch traced here: 167 us
  Pallas kernels  155 us (92%)
  local copies, waits for them, and re-layouts  10.6 us (6%)
  other arithmetic  1.84 us (1%)
    pallas_call x1, Pallas kernels, on_device(): pl.pallas_call(functools.partial(expert_kernel, n, capacity), out_shape=j...  81.8 us
    pallas_call x1, Pallas kernels, on_device(): pl.pallas_call(functools.partial(attention_kernel, n, dp), out_shape=(jax...  73 us
    unnamed x20, local copies, waits for them, and re-layouts  9.42 us

profile of v2, /device:TPU:0, one launch (start us, length us, event | category | flops | bytes accessed | tf_op | source)
XLA Modules:
  0.0 167.3 jit_solution(15181824560765901135)
XLA Ops:
  0.0 0.7 convert_bitcast_fusion
  0.7 0.7 pad_maximum_fusion.1
  1.4 0.1 copy.22
  1.5 0.0 copy-start.1
  1.5 0.1 broadcast_multiply_fusion.1
  1.6 0.3 sine_multiply_fusion
  2.0 1.0 copy_bitcast_fusion.1
  3.0 1.2 copy.26
  4.2 0.0 copy-start.2
  4.2 1.0 copy-done.2
  5.2 0.0 copy-start.4
  5.2 0.9 copy-done.4
  6.2 0.0 copy-start.6
  6.2 0.7 copy-done.6
  6.9 0.7 copy-done.7
  7.5 0.7 copy-done.8
  8.2 73.0 %attention.1 = (f32[128,2048]{1,0:T(8,128)S(1)}, bf16[128,2048]{1,0:T(8,128)(2,1)S(1)}, f32[128,128]{1,0:T(8,128)S(1)}) custom-call(bf16[16,128,128]{2,1,0:T(8,128)(2,1)S(1)} %bitcast.21, bf16[4,128,128]{2,1,0:T(8,128)(2,1)S(1)} %get-tuple-element.18.k_ref, bf16[4,128,128]{2,1,0:T(8,128)(2,1)S(1)} %get-tuple-element.17.v_ref, f32[1,128]{1,0:T(1,128)S(1)} %bitcast.24, ...), custom_call_target="tpu_custom_call" | custom-call | tf_op jit(solution)/shard_map/attention/pallas_call | solution.py:638
  81.2 0.0 copy-start
  81.2 1.0 copy-done
  82.2 0.8 copy-done.3
  83.0 0.6 copy-done.5
  83.6 0.0 copy-done.1
  83.6 81.8 %experts.1 = bf16[128,2048]{1,0:T(8,128)(2,1)} custom-call(bf16[128,2048]{1,0:T(8,128)(2,1)} %copy-done.3, f32[128,2048]{1,0:T(8,128)} %copy-done, f32[128,128]{1,0:T(8,128)} %copy-done.1, f32[128,128]{1,0:T(8,128)} %copy-done.5, bf16[1,2048,1792]{2,1,0:T(8,128)(2,1)} %gate_hbm.1, bf16[1,2048,1792]{2,1,0:T(8,128)(2,1)} %up_hbm.1, bf16[1,1792,2048]{2,1,0:T(8,128)(2,1)} %down_hbm.1), custom_call_target="tpu_custom_call" | custom-call | tf_op jit(solution)/shard_map/experts/pallas_call | solution.py:686
  165.4 1.9 %copy.28 = bf16[1,128,2048]{2,1,0:T(8,128)(2,1)} copy(bf16[1,128,2048]{2,1,0:T(8,128)(2,1)} %bitcast.26) | data formatting | bytes 1048576
  (8 shorter events, 0.0 us)
Async XLA Ops:
  1.5 82.1 %copy-start.1 = (f32[128,128]{1,0:T(8,128)}, f32[128,128]{1,0:T(8,128)S(1)}, u32[]{:S(2)}) copy-start(f32[128,128]{1,0:T(8,128)S(1)} %pad.4.table_ref.own_ref) | copy-start | bytes 196612
  4.2 1.0 copy-start.2
  5.2 0.9 copy-start.4
  6.2 0.7 copy-start.6
  6.9 0.7 copy-start.7
  7.5 0.7 copy-start.8
  81.2 1.0 copy-start
  82.2 0.8 copy-start.3
  83.0 0.6 copy-start.5

commit v3 on v2

--- a/solution.py
+++ b/solution.py
@@ -157,9 +157,10 @@
     )
 
 
-def attention_kernel(
+def attention_part(
     n,
     dp,
+    start_loads,
     q_ref,
     k_ref,
     v_ref,
@@ -173,14 +174,17 @@
     table_ref,
     mixed_ref,
     normed_ref,
-    other_ref,
+    table,
     q_rot,
     kv,
     w_full,
     att,
     proj,
     back,
-    table,
+    res_in,
+    gains,
+    norm_in,
+    in_sem,
     x_send,
     x_recv,
     t_sem,
@@ -204,6 +208,22 @@
     row_y = mine // 2
     partner = row_y * 2 + 1 - core
 
+    w_rows = w_ref.shape[0]
+    my_w = pl.ds(pl.multiple_of(me * w_rows, w_rows), w_rows)
+    fetches = [
+        pltpu.make_async_copy(src, dst, in_sem.at[i])
+        for i, (src, dst) in enumerate(
+            (
+                (kg_ref, gains.at[0]),
+                (qg_ref, gains.at[1]),
+                (w_ref, w_full.at[my_w]),
+                (res_ref, res_in),
+                (ng_ref, norm_in),
+            )
+        )
+    ]
+    for fetch in fetches:
+        fetch.start()
     barrier = pltpu.get_barrier_semaphore()
     for d in range(1, n):
         pl.semaphore_signal(
@@ -217,14 +237,11 @@
     cosine = cos_ref[...]
     sine = sin_ref[...]
     my_rows = pl.ds(pl.multiple_of(me * rows, rows), rows)
+    fetches[0].wait()
     for g in range(kv_heads):
-        kv[g, my_rows, :] = turn(k_ref[g], kg_ref[...], cosine, sine)
+        kv[g, my_rows, :] = turn(k_ref[g], gains[0], cosine, sine)
         kv[kv_heads + g, my_rows, :] = v_ref[g]
     pl.semaphore_wait(barrier, n - 1 + dp - 1)
-
-    w_rows = w_ref.shape[0]
-    my_w = pl.ds(pl.multiple_of(me * w_rows, w_rows), w_rows)
-    w_full[my_w] = w_ref[...]
 
     def key_block(s):
         return kv.at[pl.ds(0, kv_heads), pl.ds(pl.multiple_of(s * rows, rows), rows), :]
@@ -258,8 +275,11 @@
     for spread in attention_gather:
         spread.begin()
 
+    start_loads()
+    fetches[1].wait()
+
     def turn_head(h, carry):
-        q_rot[h] = turn(q_ref[h], qg_ref[...], cosine, sine)
+        q_rot[h] = turn(q_ref[h], gains[1], cosine, sine)
         return carry
 
     lax.fori_loop(0, heads, turn_head, 0)
@@ -268,8 +288,10 @@
     for t in range(1, steps):
         for spread in attention_gather:
             spread.step(t)
-    for spread in weight_gather:
-        spread.begin()
+        if t == 1:
+            fetches[2].wait()
+            for spread in weight_gather:
+                spread.begin()
     attention_gather[1].finish()
 
     per_step = 2
@@ -380,7 +402,8 @@
     for spread in attention_gather + weight_gather:
         spread.drain()
     table_copy.wait()
-    other_ref[...] = table[...]
+    fetches[3].wait()
+    fetches[4].wait()
     for copy in pair_copies:
         copy.wait_send()
     for j in range(1, ny):
@@ -393,25 +416,23 @@
     square = jnp.zeros((rows, 1), F32)
     for s in range(dp):
         cols = slice(s * block, (s + 1) * block)
-        part = res_ref[:, cols].astype(F32) + back[s].astype(F32)
+        part = res_in[:, cols].astype(F32) + back[s].astype(F32)
         mixed_ref[:, cols] = part
         square = square + jnp.sum(part * part, axis=-1, keepdims=True)
     factor = lax.rsqrt(square / model + EPS)
     for s in range(dp):
         cols = slice(s * block, (s + 1) * block)
-        normed_ref[:, cols] = (mixed_ref[:, cols] * factor * ng_ref[:, cols]).astype(BF16)
-
-
-def expert_kernel(
+        normed_ref[:, cols] = (mixed_ref[:, cols] * factor * norm_in[:, cols]).astype(BF16)
+
+
+def expert_part(
     n,
     capacity,
     normed_ref,
     mixed_ref,
     own_ref,
     other_ref,
-    gate_hbm,
-    up_hbm,
-    down_hbm,
+    loads,
     out_ref,
     gate,
     up,
@@ -425,7 +446,6 @@
     part,
     home,
     hold,
-    load_sem,
     relay_sem,
     home_sem,
     go_send,
@@ -442,20 +462,9 @@
     few = rows // 2
     slots = half * capacity
     ff = gate.shape[1]
-    loads = [
-        pltpu.make_async_copy(src.at[0], dst, load_sem.at[i])
-        for i, (src, dst) in enumerate(((gate_hbm, gate), (up_hbm, up), (down_hbm, down)))
-    ]
 
     def peer(k):
         return base + lax.rem(mine + k, half)
-
-    barrier = pltpu.get_barrier_semaphore()
-    for target in [partner] + [peer(k) for k in range(1, half)]:
-        pl.semaphore_signal(barrier, inc=1, device_id={"sp": target}, device_id_type=MESH)
-    for load in loads:
-        load.start()
-    pl.semaphore_wait(barrier, half)
 
     relays = []
     for b in range(2):
@@ -601,6 +610,26 @@
         for k in range(1, half):
             go[r, k].wait_send()
             back[r, k].wait_send()
+
+
+def layer_kernel(n, dp, capacity, *refs):
+    inputs, refs = refs[:11], refs[11:]
+    weights, out_ref, refs = refs[:3], refs[3], refs[4:]
+    middle, refs = refs[:3], refs[3:]
+    attention, refs = refs[:21], refs[21:]
+    load_sem, stores, experts = refs[0], refs[1:4], refs[4:]
+    loads = [
+        pltpu.make_async_copy(src.at[0], dst, load_sem.at[i])
+        for i, (src, dst) in enumerate(zip(weights, stores))
+    ]
+
+    def start_loads():
+        for load in loads:
+            load.start()
+
+    attention_part(n, dp, start_loads, *inputs, *middle, *attention)
+    mixed, normed, other = middle
+    expert_part(n, capacity, normed, mixed, inputs[10], other, loads, out_ref, *stores, *experts)
 
 
 def on_device(
@@ -635,39 +664,65 @@
     w_rows, w_cols = out_weight.shape
     dma = pltpu.SemaphoreType.DMA
     ny = dp // 2
-    mixed, normed, other = pl.pallas_call(
-        functools.partial(attention_kernel, n, dp),
-        out_shape=(
-            jax.ShapeDtypeStruct((rows, model), F32),
-            jax.ShapeDtypeStruct((rows, model), BF16),
-            jax.ShapeDtypeStruct(table.shape, F32),
-        ),
-        in_specs=[VMEM] * 11,
-        out_specs=(VMEM, VMEM, VMEM),
+    ff = expert_gate.shape[2]
+    few = rows // 2
+    attention_scratch = [
+        pltpu.VMEM((heads, rows, width), BF16),
+        pltpu.VMEM((2 * kv_heads, length, width), BF16),
+        pltpu.VMEM((w_rows * n, w_cols), BF16),
+        pltpu.VMEM((dp, rows, model), BF16),
+        pltpu.VMEM((dp, rows, w_cols), BF16),
+        pltpu.VMEM((dp, rows, w_cols), BF16),
+        pltpu.VMEM((rows, model), BF16),
+        pltpu.VMEM((2, 1, width), F32),
+        pltpu.VMEM((1, model), F32),
+        dma((5,)),
+        dma((4, n, 1 + x_width)),
+        dma((4, n)),
+        dma((2,)),
+        dma((ny, kv_heads)),
+        dma((ny, kv_heads)),
+        dma((kv_heads,)),
+        dma((kv_heads,)),
+        dma((ny, kv_heads)),
+        dma((ny, kv_heads)),
+        dma((dp,)),
+        dma((dp,)),
+    ]
+    result = pl.pallas_call(
+        functools.partial(layer_kernel, n, dp, capacity),
+        out_shape=jax.ShapeDtypeStruct((rows, model), BF16),
+        in_specs=[VMEM, VMEM, VMEM, ANY, ANY, VMEM, VMEM, ANY, ANY, ANY, VMEM] + [ANY] * 3,
+        out_specs=VMEM,
         scratch_shapes=[
-            pltpu.VMEM((heads, rows, width), BF16),
-            pltpu.VMEM((2 * kv_heads, length, width), BF16),
-            pltpu.VMEM((w_rows * n, w_cols), BF16),
-            pltpu.VMEM((dp, rows, model), BF16),
-            pltpu.VMEM((dp, rows, w_cols), BF16),
-            pltpu.VMEM((dp, rows, w_cols), BF16),
+            pltpu.VMEM((rows, model), F32),
+            pltpu.VMEM((rows, model), BF16),
             pltpu.VMEM(table.shape, F32),
-            dma((4, n, 1 + x_width)),
+            *attention_scratch,
+            dma((3,)),
+            pltpu.VMEM((model, ff), BF16),
+            pltpu.VMEM((model, ff), BF16),
+            pltpu.VMEM((ff, model), BF16),
+            pltpu.VMEM((2, few, model), BF16),
+            pltpu.VMEM((4, slots, model), BF16),
+            pltpu.VMEM((4, slots, model), BF16),
+            pltpu.VMEM((slots, ff), BF16),
+            pltpu.VMEM((4, slots, model), BF16),
+            pltpu.VMEM((4, slots, model), BF16),
+            pltpu.VMEM((rows, model), BF16),
+            pltpu.VMEM((2, few, model), BF16),
+            pltpu.VMEM((rows, model), F32),
+            dma((2, 2)),
+            dma((2, 2)),
             dma((4, n)),
-            dma((2,)),
-            dma((ny, kv_heads)),
-            dma((ny, kv_heads)),
-            dma((kv_heads,)),
-            dma((kv_heads,)),
-            dma((ny, kv_heads)),
-            dma((ny, kv_heads)),
-            dma((dp,)),
-            dma((dp,)),
+            dma((4, n)),
+            dma((4, n)),
+            dma((4, n)),
         ],
         compiler_params=pltpu.CompilerParams(
-            collective_id=0, has_side_effects=True, vmem_limit_bytes=40 * 1024 * 1024
+            collective_id=0, has_side_effects=True, vmem_limit_bytes=56 * 1024 * 1024
         ),
-        name="attention",
+        name="layer",
     )(
         queries[0].transpose(1, 0, 2),
         key_rows[0].transpose(1, 0, 2),
@@ -680,40 +735,10 @@
         residual[0],
         norm_gain[None],
         table,
-    )
-    ff = expert_gate.shape[2]
-    few = rows // 2
-    result = pl.pallas_call(
-        functools.partial(expert_kernel, n, capacity),
-        out_shape=jax.ShapeDtypeStruct((rows, model), BF16),
-        in_specs=[VMEM, VMEM, VMEM, VMEM, ANY, ANY, ANY],
-        out_specs=VMEM,
-        scratch_shapes=[
-            pltpu.VMEM((model, ff), BF16),
-            pltpu.VMEM((model, ff), BF16),
-            pltpu.VMEM((ff, model), BF16),
-            pltpu.VMEM((2, few, model), BF16),
-            pltpu.VMEM((4, slots, model), BF16),
-            pltpu.VMEM((4, slots, model), BF16),
-            pltpu.VMEM((slots, ff), BF16),
-            pltpu.VMEM((4, slots, model), BF16),
-            pltpu.VMEM((4, slots, model), BF16),
-            pltpu.VMEM((rows, model), BF16),
-            pltpu.VMEM((2, few, model), BF16),
-            pltpu.VMEM((rows, model), F32),
-            dma((3,)),
-            dma((2, 2)),
-            dma((2, 2)),
-            dma((4, n)),
-            dma((4, n)),
-            dma((4, n)),
-            dma((4, n)),
-        ],
-        compiler_params=pltpu.CompilerParams(
-            collective_id=1, has_side_effects=True, vmem_limit_bytes=56 * 1024 * 1024
-        ),
-        name="experts",
-    )(normed, mixed, table, other, expert_gate, expert_up, expert_down)
+        expert_gate,
+        expert_up,
+        expert_down,
+    )
     return result[None]
 
 

time: 168 us -> 164 us (0.976)
  local copies, waits for them, and re-layouts: 10.6 us -> 6.3 us
    unnamed x20 -> x2, local copies, waits for them, and re-layouts: 9.42 us -> 3.85 us
    pallas_call x2 -> x1, Pallas kernels: 155 us -> 155 us  [on_device(): pl.pallas_call(functools.partial(layer_kernel, n, dp, capacity), out_shap...]
where the time goes in v3:
time: 164 us
  Pallas kernels  155 us (95%)
  local copies, waits for them, and re-layouts  6.3 us (4%)
  other arithmetic  2.48 us (2%)
    pallas_call x1, Pallas kernels, on_device(): pl.pallas_call(functools.partial(layer_kernel, n, dp, capacity), out_shap...  155 us
    unnamed x2, local copies, waits for them, and re-layouts  3.85 us

profile of v3, /device:TPU:0, one launch (start us, length us, event | category | flops | bytes accessed | tf_op | source)
XLA Modules:
  0.0 163.9 jit_solution(4983028714243170640)
XLA Ops:
  0.0 0.7 convert_bitcast_fusion
  0.7 0.7 pad_maximum_fusion.1
  1.4 0.1 copy.22
  1.5 0.6 pad.4.refs_10_
  2.2 0.1 broadcast_multiply_fusion.1
  2.3 1.0 sine_multiply_fusion
  3.3 1.7 %copy_bitcast_fusion.1 = (bf16[4,128,128]{2,1,0:T(8,128)(2,1)}, bf16[4,128,128]{2,1,0:T(8,128)(2,1)}) fusion(bf16[1,128,4,128]{3,2,1,0:T(4,128)(2,1)} %param.15, bf16[1,128,4,128]{3,2,1,0:T(4,128)(2,1)} %param.14), kind=kLoop, calls=%fused_computation.1 | loop fusion | bytes 524288 | tf_op jit(solution)/shard_map/transpose | solution.py:729
  5.0 2.0 %copy.26 = bf16[1,128,16,128]{3,1,2,0:T(8,128)(2,1)} copy(bf16[1,128,16,128]{3,2,1,0:T(8,128)(2,1)} %param.13) | data formatting | bytes 1048576 | tf_op args[0]
  6.9 155.1 %layer.1 = bf16[128,2048]{1,0:T(8,128)(2,1)} custom-call(bf16[16,128,128]{2,1,0:T(8,128)(2,1)} %bitcast.22, bf16[4,128,128]{2,1,0:T(8,128)(2,1)} %get-tuple-element.12.refs_1_, bf16[4,128,128]{2,1,0:T(8,128)(2,1)} %get-tuple-element.11.refs_2_, f32[1,128]{1,0:T(1,128)} %bitcast.26, f32[1,128]{1,0:T(1,128)} %bitcast.27, f32[128,128]{1,0:T(8,128)} %get-tuple-element.6.refs_5_, ...), custom_call_target="tpu_custom_call" | custom-call | tf_op jit(solution)/shard_map/layer/pallas_call | solution.py:692
  162.0 1.9 %copy.28 = bf16[1,128,2048]{2,1,0:T(8,128)(2,1)} copy(bf16[1,128,2048]{2,1,0:T(8,128)(2,1)} %bitcast.21) | data formatting | bytes 1048576
  (3 shorter events, 0.0 us)

commit v4 on v3

--- a/solution.py
+++ b/solution.py
@@ -584,18 +584,18 @@
         hold[lines, cols] = mixed_ref[lines, cols] + value
 
     dispatch(0)
-    dispatch(1)
     loads[0].wait()
     loads[1].wait()
     serve(0)
     relays[0].wait_recv()
     dispatch(2)
-    serve(1)
+    dispatch(1)
     relays[1].wait_recv()
     dispatch(3)
     serve(2)
     serve(3)
     send_home(0)
+    serve(1)
     send_home(1)
     combine(0, store_own)
     combine(1, store_own)

time: 164 us -> 166 us (1.012)
  Pallas kernels: 155 us -> 157 us
where the time goes in v4:
time: 166 us; the launch traced here: 165 us
  Pallas kernels  157 us (95%)
  local copies, waits for them, and re-layouts  6.3 us (4%)
  other arithmetic  2.48 us (1%)
    pallas_call x1, Pallas kernels, on_device(): pl.pallas_call(functools.partial(layer_kernel, n, dp, capacity), out_shap...  157 us
    unnamed x2, local copies, waits for them, and re-layouts  3.85 us

profile of v4, /device:TPU:0, one launch (start us, length us, event | category | flops | bytes accessed | tf_op | source)
XLA Modules:
  0.0 165.4 jit_solution(1288879864059164386)
XLA Ops:
  0.0 0.7 convert_bitcast_fusion
  0.7 0.7 pad_maximum_fusion.1
  1.4 0.1 copy.22
  1.5 0.6 pad.4.refs_10_
  2.2 0.1 broadcast_multiply_fusion.1
  2.3 1.0 sine_multiply_fusion
  3.3 1.7 %copy_bitcast_fusion.1 = (bf16[4,128,128]{2,1,0:T(8,128)(2,1)}, bf16[4,128,128]{2,1,0:T(8,128)(2,1)}) fusion(bf16[1,128,4,128]{3,2,1,0:T(4,128)(2,1)} %param.15, bf16[1,128,4,128]{3,2,1,0:T(4,128)(2,1)} %param.14), kind=kLoop, calls=%fused_computation.1 | loop fusion | bytes 524288 | tf_op jit(solution)/shard_map/transpose | solution.py:729
  5.0 2.0 %copy.26 = bf16[1,128,16,128]{3,1,2,0:T(8,128)(2,1)} copy(bf16[1,128,16,128]{3,2,1,0:T(8,128)(2,1)} %param.13) | data formatting | bytes 1048576 | tf_op args[0]
  6.9 156.6 %layer.1 = bf16[128,2048]{1,0:T(8,128)(2,1)} custom-call(bf16[16,128,128]{2,1,0:T(8,128)(2,1)} %bitcast.22, bf16[4,128,128]{2,1,0:T(8,128)(2,1)} %get-tuple-element.12.refs_1_, bf16[4,128,128]{2,1,0:T(8,128)(2,1)} %get-tuple-element.11.refs_2_, f32[1,128]{1,0:T(1,128)} %bitcast.26, f32[1,128]{1,0:T(1,128)} %bitcast.27, f32[128,128]{1,0:T(8,128)} %get-tuple-element.6.refs_5_, ...), custom_call_target="tpu_custom_call" | custom-call | tf_op jit(solution)/shard_map/layer/pallas_call | solution.py:692
  163.5 1.9 %copy.28 = bf16[1,128,2048]{2,1,0:T(8,128)(2,1)} copy(bf16[1,128,2048]{2,1,0:T(8,128)(2,1)} %bitcast.21) | data formatting | bytes 1048576
  (3 shorter events, 0.0 us)
